TPU v7x, 32 devices: a whole 2x2x4 slice. The times are simulated.
32 devices in a mesh: ep: 4 (over z), tp: 8 (over y, x, core).
Axes of the slice: x: 2, y: 2, z: 4, core: 2. Of those that a mesh axis runs over, the one named last changes fastest.
Arguments:
- tokens: bfloat16 [4096, 2048], P(('ep', 'tp')), may hold values from -40 to 40
- norm_gain: float32 [2048], replicated, may hold values from 0.1 to 1.9
- routes: int32 [4096, 2], P(('ep', 'tp')), may hold values from 0 to 7, all different within a row; in each aligned block of 128 rows (0 to 127, 128 to 255, ...) at most 64 rows name the same one
- gates: float32 [4096, 2], P(('ep', 'tp')), may hold values from 0.25 to 2
- expert_gate: bfloat16 [8, 2048, 512], P('tp'), may hold values from -0.125 to 0.125
- expert_up: bfloat16 [8, 2048, 512], P('tp'), may hold values from -0.125 to 0.125
- expert_down: bfloat16 [8, 512, 2048], P('tp'), may hold values from -0.25 to 0.25
- shared_gate: bfloat16 [2048, 256], replicated, may hold values from -0.125 to 0.125
- shared_up: bfloat16 [2048, 256], replicated, may hold values from -0.125 to 0.125
- shared_down: bfloat16 [256, 2048], replicated, may hold values from -0.375 to 0.375
Outputs:
- mixed: bfloat16 [4096, 2048], P(('ep', 'tp'))
- load: float32 [8], replicated
Inputs may be any that keep to these rules, and one draw needn't show every extreme that they name: `routes`: each row names 2 different experts. Among the rows of one device no expert is named by more than 64 rows, and in every draw some expert is named by exactly 64 rows of some device.
All inputs are finite; a program needn't handle non-finite values.
Results may differ from a plain program's by a relative error of at most 0.002.
The roundings to bfloat16 on the way count: a program that leaves them out, or rounds other values in their place, can miss the bound.
Values may be sent and summed in bfloat16 or wider, within the bound.
A program may use at most 64 MiB of HBM per device.

v0:
```python
import jax
import jax.numpy as jnp
from jax import lax
from jax.sharding import PartitionSpec as P


def layer_normed(token_block, norm_gain):
    values = token_block.astype(jnp.float32)
    center = jnp.mean(values, axis=-1, keepdims=True)
    spread = jnp.mean(jnp.square(values - center), axis=-1, keepdims=True)
    return ((values - center) * lax.rsqrt(spread + 1e-05) * norm_gain).astype(jnp.bfloat16)


def gated_mlp(row_block, w_gate, w_up, w_down):
    gate_part = jnp.dot(row_block, w_gate, preferred_element_type=jnp.float32)
    up_part = jnp.dot(row_block, w_up, preferred_element_type=jnp.float32)
    hidden = (jax.nn.silu(gate_part) * up_part).astype(jnp.bfloat16)
    return jnp.dot(hidden, w_down, preferred_element_type=jnp.float32)


def per_device(
    tokens,
    norm_gain,
    routes,
    gates,
    expert_gate,
    expert_up,
    expert_down,
    shared_gate,
    shared_up,
    shared_down,
):
    normed = layer_normed(tokens, norm_gain)
    count_rows, feature_count = normed.shape
    top_count = routes.shape[1]
    groups = lax.axis_size("tp")
    devices = lax.axis_size("ep") * groups
    capacity = 2 * count_rows * top_count // groups
    flat_expert = routes.reshape(-1)
    onehot = (flat_expert[:, None] == jnp.arange(groups, dtype=jnp.int32)[None, :]).astype(
        jnp.int32
    )
    earlier = jnp.cumsum(onehot, axis=0) - onehot
    slot_index = jnp.sum(earlier * onehot, axis=1)
    destination = flat_expert * capacity + slot_index
    local_counts = jnp.sum(onehot, axis=0).astype(jnp.float32)
    copies = jnp.repeat(normed, top_count, axis=0)
    outgoing = (
        jnp.zeros((groups * capacity, feature_count), jnp.bfloat16).at[destination].set(copies)
    )
    outgoing = outgoing.reshape(groups, capacity, feature_count)
    arrived = lax.all_to_all(outgoing, "tp", split_axis=0, concat_axis=0, tiled=True)
    sources, slot_count, _ = arrived.shape
    result = gated_mlp(
        arrived.reshape(sources * slot_count, feature_count),
        expert_gate[0],
        expert_up[0],
        expert_down[0],
    )
    result = result.astype(jnp.bfloat16).reshape(sources, slot_count, feature_count)
    returned = lax.all_to_all(result, "tp", split_axis=0, concat_axis=0, tiled=True)
    flat_returned = returned.reshape(groups * capacity, feature_count)
    per_copy = flat_returned[destination].reshape(count_rows, top_count, feature_count)
    routed = jnp.sum(gates[:, :, None] * per_copy.astype(jnp.float32), axis=1)
    shared_out = gated_mlp(normed, shared_gate, shared_up, shared_down)
    mixed = (routed + shared_out).astype(jnp.bfloat16)
    total_counts = lax.psum(local_counts, ("ep", "tp"))
    load = total_counts * (groups / (count_rows * top_count * devices))
    return (mixed, load)


def solution(mesh):
    placed = (
        P(("ep", "tp"), None),
        P(),
        P(("ep", "tp"), None),
        P(("ep", "tp"), None),
        P("tp", None, None),
        P("tp", None, None),
        P("tp", None, None),
        P(),
        P(),
        P(),
    )
    return jax.shard_map(
        per_device,
        mesh=mesh,
        in_specs=placed,
        out_specs=(P(("ep", "tp"), None), P()),
        check_vma=False,
    )
```

profile of v0, /device:TPU:0, one launch (start us, length us, event | category | flops | bytes accessed | tf_op | source)
XLA Modules:
  0.0 142.1 jit_solution(17562173664722931788)
XLA Ops:
  0.6 0.0 copy-start
  0.6 0.9 copy.15
  1.6 0.1 eq.29
  1.7 0.1 eq.25
  1.9 0.7 broadcast_multiply_fusion
  2.6 0.6 reduce-window.6
  3.1 0.2 slice_reduce_fusion
  3.4 0.1 copy.14
  3.5 0.1 mul.63
  3.6 1.2 convert_reduce_fusion
  4.8 1.3 fusion.15
  6.2 1.4 fusion.17
  7.6 1.6 %broadcast_in_dim.5 = bf16[128,2,2048]{2,1,0:T(2,128)(2,1)} broadcast(bf16[128,2048]{1,0:T(8,128)(2,1)S(1)} %fusion.17), dimensions={0,2} | broadcast | bytes 1572864 | tf_op jit(solution)/shard_map/broadcast_in_dim | solution.py:47
  9.2 2.3 %reshape.101 = bf16[256,2048]{1,0:T(8,128)(2,1)} reshape(bf16[128,2,2048]{2,1,0:T(2,128)(2,1)} %broadcast_in_dim.5) | data formatting | bytes 2097152 | tf_op jit(solution)/shard_map/reshape | solution.py:47
  11.5 0.1 convert_reduce_fusion.1
  11.6 4.4 %scatter_custom_fusion = bf16[512,2048]{1,0:T(8,128)(2,1)} fusion(s32[256]{0:T(256)S(1)} %bitcast.36, bf16[256,2048]{1,0:T(8,128)(2,1)} %reshape.101, bf16[]{:T(256)} %constant.9.clone.1), kind=kCustom, calls=%fused_computation.22 | custom fusion | bytes 2097664 | tf_op jit(solution)/shard_map/scatter | solution.py:49
  16.1 0.0 copy-start.3
  16.1 31.9 %all_to_all.10 = bf16[8,64,2048]{2,1,0:T(8,128)(2,1)S(1)} all-to-all(bf16[8,64,2048]{2,1,0:T(8,128)(2,1)} %bitcast.32), channel_id=1, replica_groups=mesh['ep'=4,'tp'=8] {'tp'}, dimensions={0} | all-to-all | bytes 4194304 | tf_op jit(solution)/shard_map/all_to_all | solution.py:52
  48.0 0.0 copy-start.1
  48.0 1.3 copy-done.1
  49.3 0.0 copy-done.3
  49.3 2.2 %fusion.4 = f32[512,512]{1,0:T(8,128)} fusion(bf16[512,2048]{1,0:T(8,128)(2,1)S(1)} %bitcast.34, bf16[1,2048,512]{2,1,0:T(8,128)(2,1)S(1)} %copy-done.3), kind=kOutput, calls=%fused_computation.8 | convolution fusion | flops 1073741824 | bytes 5242880 | tf_op jit(solution)/shard_map/dot_general | solution.py:15
  51.5 0.0 copy-done
  51.5 6.3 %convolution_convert_fusion = bf16[512,2048]{1,0:T(8,128)(2,1)} fusion(bf16[1,512,2048]{2,1,0:T(8,128)(2,1)S(1)} %copy-done, bf16[512,2048]{1,0:T(8,128)(2,1)} %bitcast.35, bf16[1,2048,512]{2,1,0:T(8,128)(2,1)} %param.15, f32[512,512]{1,0:T(8,128)} %fusion.4), kind=kOutput, calls=%fused_computation.2 | convolution fusion | flops 2150105088 | bytes 9437184 | tf_op jit(solution)/shard_map/dot_general | solution.py:18
  57.8 0.0 copy-start.2
  57.8 4.5 %all-to-all-start.1 = ((bf16[8,64,2048]{2,1,0:T(8,128)(2,1)}), bf16[8,64,2048]{2,1,0:T(8,128)(2,1)}, u32[]{:S(2)}, u32[]{:S(2)}) async-start(bf16[8,64,2048]{2,1,0:T(8,128)(2,1)} %bitcast.33), calls=%async_computation.1 | async-start | bytes 4194304 | tf_op jit(solution)/shard_map/all_to_all | solution.py:61
  62.3 59.9 %psum.7 = f32[8]{0:T(128)S(1)} all-reduce(f32[8]{0:T(128)S(1)} %convert_element_type.44), channel_id=1, replica_groups=mesh['ep'=4,'tp'=8] {'ep','tp'}, use_global_device_ids=true, to_apply=%region_8.9 | all-reduce | flops 8 | bytes 64 | tf_op jit(solution)/shard_map/psum | solution.py:67
  122.2 0.0 copy-done.2
  122.2 0.1 copy.13
  122.3 0.5 broadcast_multiply_fusion.1
  122.8 1.5 %fusion.34 = f32[128,256]{1,0:T(8,128)S(1)} fusion(bf16[128,2048]{1,0:T(8,128)(2,1)S(1)} %fusion.17, bf16[2048,256]{1,0:T(8,128)(2,1)} %param.17), kind=kOutput, calls=%fused_computation.47 | convolution fusion | flops 134217728 | bytes 1703936 | tf_op jit(solution)/shard_map/dot_general | solution.py:15
  124.4 0.0 all-to-all-done.1
  124.4 5.2 %gather_fusion = bf16[256,2048]{1,0:T(8,128)(2,1)} fusion(bf16[512,2048]{1,0:T(8,128)(2,1)} %bitcast.10, s32[1024]{0:T(1024)S(1)} %pad_clamp_fusion), kind=kCustom, calls=%fused_computation | custom fusion | bytes 2098176 | tf_op jit(solution)/shard_map/gather | solution.py:63
  129.6 3.4 %reshape.88 = f32[128,2,2048]{2,1,0:T(2,128)} reshape(bf16[256,2048]{1,0:T(8,128)(2,1)} %gather_fusion) | data formatting | bytes 3145728 | tf_op jit(solution)/shard_map/convert_element_type | solution.py:64
  133.0 5.7 %multiply_reduce_fusion = f32[128,2048]{1,0:T(8,128)} fusion(f32[128,2,2048]{2,1,0:T(2,128)} %reshape.88, f32[128,2]{1,0:T(8,128)S(1)} %copy.13), kind=kLoop, calls=%fused_computation.10 | loop fusion | flops 786432 | bytes 3146752 | tf_op jit(solution)/shard_map/reduce_sum | solution.py:64
  138.7 3.4 %fusion = bf16[128,2048]{1,0:T(8,128)(2,1)} fusion(f32[128,2048]{1,0:T(8,128)} %multiply_reduce_fusion, bf16[256,2048]{1,0:T(8,128)(2,1)} %param.19, bf16[128,2048]{1,0:T(8,128)(2,1)S(1)} %fusion.17, bf16[2048,256]{1,0:T(8,128)(2,1)} %param.18, f32[128,256]{1,0:T(8,128)S(1)} %fusion.34), kind=kOutput, calls=%fused_computation.4 | convolution fusion | flops 269156352 | bytes 4325376 | tf_op jit(solution)/shard_map/dot_general | solution.py:18
  (8 shorter events, 0.1 us)
Async XLA Ops:
  0.6 50.9 %copy-start = (bf16[1,512,2048]{2,1,0:T(8,128)(2,1)S(1)}, bf16[1,512,2048]{2,1,0:T(8,128)(2,1)}, u32[]{:S(2)}) copy-start(bf16[1,512,2048]{2,1,0:T(8,128)(2,1)} %param.16) | copy-start | bytes 6291460
  16.1 33.2 %copy-start.3 = (bf16[1,2048,512]{2,1,0:T(8,128)(2,1)S(1)}, bf16[1,2048,512]{2,1,0:T(8,128)(2,1)}, u32[]{:S(2)}) copy-start(bf16[1,2048,512]{2,1,0:T(8,128)(2,1)} %param.14) | copy-start | bytes 6291460
  48.0 1.3 copy-start.1
  57.8 64.4 %copy-start.2 = (f32[128,2]{0,1:T(2,128)S(1)}, f32[128,2]{0,1:T(2,128)}, u32[]{:S(2)}) copy-start(f32[128,2]{0,1:T(2,128)} %param.13) | copy-start | bytes 3076
  57.8 66.6 %all-to-all-start.1 = ((bf16[8,64,2048]{2,1,0:T(8,128)(2,1)}), bf16[8,64,2048]{2,1,0:T(8,128)(2,1)}, u32[]{:S(2)}, u32[]{:S(2)}) async-start(bf16[8,64,2048]{2,1,0:T(8,128)(2,1)} %bitcast.33), calls=%async_computation.1 | async-start | bytes 4194304 | tf_op jit(solution)/shard_map/all_to_all | solution.py:61
where the time goes:
time: 143 us; the launch traced here: 142 us
  blocking collectives  91.8 us (64%)
  local copies, waits for them, and re-layouts  20 us (14%)
  matrix products  13.5 us (9%)
  other arithmetic  11.6 us (8%)
  starting transfers between devices  4.5 us (3%)
    psum x1, blocking collectives, per_device(): total_counts = lax.psum(local_counts, ('ep', 'tp'))  59.9 us
    all_to_all x1, blocking collectives, per_device(): lax.all_to_all(outgoing, 'tp', split_axis=0, concat_axis=0, tiled=True)  31.9 us
    dot_general x2, matrix products, gated_mlp(): return jnp.dot(hidden, w_down, preferred_element_type=jnp.float32)  9.71 us
    reduce_sum x1, other arithmetic, per_device(): routed = jnp.sum(gates[:, :, None] * per_copy.astype(jnp.float32), axis=1)  5.72 us
    gather x1, local copies, waits for them, and re-layouts, per_device(): flat_returned[destination].reshape(count_rows, top_count, feature_count)  5.2 us
    all_to_all x1, starting transfers between devices, per_device(): lax.all_to_all(result, 'tp', split_axis=0, concat_axis=0, tiled=True)  4.5 us
    scatter x1, local copies, waits for them, and re-layouts, per_device(): jnp.zeros((groups * capacity, feature_count), jnp.bfloat16).at[destination]  4.44 us
    dot_general x2, matrix products, gated_mlp(): gate_part = jnp.dot(row_block, w_gate, preferred_element_type=jnp.float32)  3.76 us
  transfers between devices with their start and end apart: 1, of which 0 were waited for; matrix products, arithmetic and copies ran while one was open for 2% of the time, Pallas kernels for 0%

commit v1 on v0

v1 whole, which is shorter than its diff:
```python
import functools

import jax
import jax.numpy as jnp
from jax import lax
from jax.experimental import pallas as pl
from jax.experimental.pallas import tpu as pltpu
from jax.sharding import PartitionSpec as P

F32 = jnp.float32
BF16 = jnp.bfloat16


def kernel(
    n,
    eps,
    cap,
    tokens,
    routes,
    gates,
    gain,
    expert_gate,
    expert_up,
    expert_down,
    shared_gate,
    shared_up,
    shared_down,
    out,
    load,
    blocks,
    group_routes,
    every_routes,
    rows_in,
    hidden,
    results,
    returned,
    total,
    w_gate,
    w_up,
    w_down,
    s_gate,
    s_up,
    s_down,
    weight_sem,
    own_sem,
    route_send,
    route_recv,
    far_send,
    far_recv,
    token_send,
    token_recv,
    result_send,
    result_recv,
):
    me = lax.axis_index("tp")
    here = lax.axis_index("ep")
    rows, width = tokens.shape
    half = rows // 2
    chunk = rows // cap
    relay = n == 8
    order = [lax.rem(me + i, n) for i in range(n)]
    if relay:
        core, xbit, ybit = me % 2, (me // 2) % 2, me // 4
        across = 1 - 2 * core
        sib = me + across
        nx = me + 2 * (1 - 2 * xbit)
        ny = me + 4 * (1 - 2 * ybit)
        nd = nx + 4 * (1 - 2 * ybit)
        order = [me, sib, nx, nx + across, ny, ny + across, nd, nd + across]

    weights = [
        pltpu.make_async_copy(src, dst, weight_sem.at[i])
        for i, (src, dst) in enumerate(
            [
                (expert_gate.at[0], w_gate),
                (expert_up.at[0], w_up),
                (expert_down.at[0], w_down),
                (shared_gate, s_gate),
                (shared_up, s_up),
                (shared_down, s_down),
            ]
        )
    ]
    for copy in weights:
        copy.start()
    own_routes = pltpu.make_async_copy(routes, group_routes.at[me], own_sem.at[0])
    own_routes.start()

    barrier = pltpu.get_barrier_semaphore()
    planes = [lax.rem(here + i, eps) for i in range(1, eps)]
    for peer in order[1:]:
        pl.semaphore_signal(barrier, inc=1, device_id={"tp": peer})
    for plane in planes:
        pl.semaphore_signal(barrier, inc=1, device_id={"ep": plane})
    pl.semaphore_wait(barrier, n - 1 + eps - 1)

    pending = []
    for i, peer in enumerate(order[1:]):
        copy = pltpu.make_async_remote_copy(
            src_ref=routes,
            dst_ref=group_routes.at[me],
            send_sem=route_send.at[i],
            recv_sem=route_recv.at[me],
            device_id={"tp": peer},
        )
        copy.start()
        pending.append(copy)

    def part(ref, piece):
        return ref.at[pl.ds(piece * half, half)]

    def send(source, piece, slot, peer, number):
        copy = pltpu.make_async_remote_copy(
            src_ref=part(source, piece),
            dst_ref=part(blocks.at[slot], piece),
            send_sem=token_send.at[number],
            recv_sem=token_recv.at[slot, piece],
            device_id={"tp": peer},
        )
        copy.start()
        pending.append(copy)

    def landed(slot, piece):
        ref = part(blocks.at[slot], piece)
        pltpu.make_async_copy(ref, ref, token_recv.at[slot, piece]).wait()

    if relay:
        send(tokens, 0, me, nx, 0)
        send(tokens, 1, me, ny, 1)
        send(tokens, 1, me, nx, 2)
        send(tokens, 0, me, ny, 3)
        send(tokens, 0, me, sib, 4)
        send(tokens, 1, me, sib, 5)
    else:
        for i, peer in enumerate(order[1:]):
            send(tokens, 0, me, peer, 2 * i)
            send(tokens, 1, me, peer, 2 * i + 1)

    earlier = (
        lax.broadcasted_iota(jnp.int32, (rows, rows), 0)
        < lax.broadcasted_iota(jnp.int32, (rows, rows), 1)
    ).astype(BF16)
    row_in_slot = lax.broadcasted_iota(jnp.int32, (cap, rows), 0)

    def normed_of(values):
        center = jnp.mean(values, axis=-1, keepdims=True)
        values = values - center
        spread = jnp.mean(jnp.square(values), axis=-1, keepdims=True)
        return (values * lax.rsqrt(spread + 1e-05) * gain[...]).astype(BF16)

    def gated(values, gate_ref, up_ref):
        gate_part = jnp.dot(values, gate_ref[...], preferred_element_type=F32)
        up_part = jnp.dot(values, up_ref[...], preferred_element_type=F32)
        return (gate_part * (1.0 / (1.0 + jnp.exp(-gate_part))) * up_part).astype(BF16)

    def gather(number):
        for g in range(chunk):
            source = order[number * chunk + g]
            named = group_routes[source]
            member = (named[0:1] == me) | (named[1:2] == me)
            count = jnp.dot(
                jnp.broadcast_to(member.astype(F32), (8, rows)).astype(BF16),
                earlier,
                preferred_element_type=F32,
            )[0:1].astype(jnp.int32)
            slot = jnp.where(member, count, -1)
            pick = (row_in_slot == slot).astype(F32).astype(BF16)
            held = tokens[...] if number * chunk + g == 0 else blocks[source]
            taken = jnp.dot(pick, held, preferred_element_type=F32)
            rows_in[g * cap : (g + 1) * cap, :] = normed_of(taken)

    tile = 512

    def expert(number):
        hidden[...] = gated(rows_in[...], w_gate, w_up)
        for at in range(0, width, tile):
            value = jnp.dot(
                hidden[...], w_down[:, at : at + tile], preferred_element_type=F32
            ).astype(BF16)
            for g in range(chunk):
                piece = value[g * cap : (g + 1) * cap]
                if number * chunk + g == 0:
                    returned[me, :, at : at + tile] = piece
                else:
                    results[number * chunk + g, :, at : at + tile] = piece
        for g in range(chunk):
            i = number * chunk + g
            if i == 0:
                continue
            copy = pltpu.make_async_remote_copy(
                src_ref=results.at[i],
                dst_ref=returned.at[me],
                send_sem=result_send.at[i],
                recv_sem=result_recv.at[me],
                device_id={"tp": order[i]},
            )
            copy.start()
            pending.append(copy)

    own_routes.wait()
    for peer in order[1:]:
        ref = group_routes.at[peer]
        pltpu.make_async_copy(ref, ref, route_recv.at[peer]).wait()
    for i, plane in enumerate(planes):
        copy = pltpu.make_async_remote_copy(
            src_ref=group_routes,
            dst_ref=every_routes.at[here],
            send_sem=far_send.at[i],
            recv_sem=far_recv.at[here],
            device_id={"ep": plane},
        )
        copy.start()
        pending.append(copy)

    if relay:
        landed(sib, 0)
        landed(sib, 1)
        gather(0)
        landed(nx, 0)
        send(blocks.at[nx], 0, nx, ny, 6)
        send(blocks.at[nx], 0, nx, sib, 7)
        landed(ny, 1)
        send(blocks.at[ny], 1, ny, nx, 8)
        send(blocks.at[ny], 1, ny, sib, 9)
        for copy in weights[:3]:
            copy.wait()
        expert(0)
        landed(nx, 1)
        send(blocks.at[nx], 1, nx, sib, 10)
        landed(ny, 0)
        send(blocks.at[ny], 0, ny, sib, 11)
        for number in (1, 2):
            landed(order[2 * number + 1], 0)
            landed(order[2 * number + 1], 1)
            gather(number)
            expert(number)
        landed(nd, 0)
        send(blocks.at[nd], 0, nd, sib, 12)
        landed(nd, 1)
        send(blocks.at[nd], 1, nd, sib, 13)
        landed(order[7], 0)
        landed(order[7], 1)
        gather(3)
        expert(3)
    else:
        for copy in weights[:3]:
            copy.wait()
        for number in range(n // chunk):
            for source in order[max(1, number * chunk) : (number + 1) * chunk]:
                landed(source, 0)
                landed(source, 1)
            gather(number)
            expert(number)

    for copy in weights[3:]:
        copy.wait()
    rows_in[...] = normed_of(tokens[...].astype(F32))
    shared = gated(rows_in[...], s_gate, s_up)
    for at in range(0, width, tile):
        total[:, at : at + tile] = jnp.dot(
            shared, s_down[:, at : at + tile], preferred_element_type=F32
        )

    expert_ids = lax.broadcasted_iota(jnp.int32, (n, rows), 0)
    first, second = routes[0:1], routes[1:2]
    member = ((first == expert_ids) | (second == expert_ids)).astype(F32)
    ranks = jnp.dot(member.astype(BF16), earlier, preferred_element_type=F32)
    slots = [
        named * cap
        + jnp.sum(jnp.where(named == expert_ids, ranks, 0.0), axis=0, keepdims=True).astype(jnp.int32)
        for named in (first, second)
    ]

    def counted(ref_of, amount, start):
        def step(i, sums):
            named = ref_of(i)
            return (
                sums
                + (named[0:1] == expert_ids).astype(F32)
                + (named[1:2] == expert_ids).astype(F32)
            )

        return lax.fori_loop(0, amount, step, start)

    sums = counted(lambda i: group_routes[i], n, jnp.zeros((n, rows), F32))
    for plane in planes:
        ref = every_routes.at[plane]
        pltpu.make_async_copy(ref, ref, far_recv.at[plane]).wait()
        sums = counted(lambda i, plane=plane: every_routes[plane, i], n, sums)
    counts = lax.dot_general(
        jnp.ones((8, rows), F32),
        sums,
        (((1,), (1,)), ((), ())),
        precision=lax.Precision.HIGHEST,
        preferred_element_type=F32,
    )
    load[...] = counts[0:1, :] * (n / (rows * 2 * n * eps))

    gate_of = [gates[:, k : k + 1] for k in range(2)]
    for number in range(n // chunk):
        sources = order[number * chunk : (number + 1) * chunk]
        for g, source in enumerate(sources):
            if number * chunk + g > 0:
                ref = returned.at[source]
                pltpu.make_async_copy(ref, ref, result_recv.at[source]).wait()
        picks = [
            jnp.transpose(
                jnp.concatenate(
                    [(row_in_slot + source * cap == slot).astype(F32) for source in sources], axis=0
                )
            ).astype(BF16)
            for slot in slots
        ]
        last = number == n // chunk - 1
        for at in range(0, width, tile):
            back = jnp.concatenate([returned[source, :, at : at + tile] for source in sources], axis=0)
            value = total[:, at : at + tile]
            for k in range(2):
                value = value + gate_of[k] * jnp.dot(picks[k], back, preferred_element_type=F32)
            if last:
                out[:, at : at + tile] = value.astype(BF16)
            else:
                total[:, at : at + tile] = value

    for copy in pending:
        copy.wait_send()


def per_device(
    tokens,
    norm_gain,
    routes,
    gates,
    expert_gate,
    expert_up,
    expert_down,
    shared_gate,
    shared_up,
    shared_down,
):
    n, eps = lax.axis_size("tp"), lax.axis_size("ep")
    rows, width = tokens.shape
    top = routes.shape[1]
    cap = 2 * rows * top // n
    units = expert_gate.shape[2]
    sends = 14 if n == 8 else 2 * (n - 1)
    vmem = pl.BlockSpec(memory_space=pltpu.VMEM)
    hbm = pl.BlockSpec(memory_space=pl.ANY)
    dma = pltpu.SemaphoreType.DMA
    mixed, load = pl.pallas_call(
        functools.partial(kernel, n, eps, cap),
        out_shape=(
            jax.ShapeDtypeStruct((rows, width), BF16),
            jax.ShapeDtypeStruct((1, n), F32),
        ),
        in_specs=[vmem] * 4 + [hbm] * 6,
        out_specs=(vmem, vmem),
        scratch_shapes=[
            pltpu.VMEM((n, rows, width), BF16),
            pltpu.VMEM((n, top, rows), jnp.int32),
            pltpu.VMEM((eps, n, top, rows), jnp.int32),
            pltpu.VMEM((rows, width), BF16),
            pltpu.VMEM((rows, units), BF16),
            pltpu.VMEM((n, cap, width), BF16),
            pltpu.VMEM((n, cap, width), BF16),
            pltpu.VMEM((rows, width), F32),
            pltpu.VMEM(expert_gate.shape[1:], BF16),
            pltpu.VMEM(expert_up.shape[1:], BF16),
            pltpu.VMEM(expert_down.shape[1:], BF16),
            pltpu.VMEM(shared_gate.shape, BF16),
            pltpu.VMEM(shared_up.shape, BF16),
            pltpu.VMEM(shared_down.shape, BF16),
            dma((6,)),
            dma((1,)),
            dma((n - 1,)),
            dma((n,)),
            dma((max(1, eps - 1),)),
            dma((eps,)),
            dma((sends,)),
            dma((n, 2)),
            dma((n,)),
            dma((n,)),
        ],
        compiler_params=pltpu.CompilerParams(collective_id=0, has_side_effects=True),
    )(
        tokens,
        routes.T,
        gates,
        norm_gain.reshape(1, width),
        expert_gate,
        expert_up,
        expert_down,
        shared_gate,
        shared_up,
        shared_down,
    )
    return mixed, load.reshape(n)


def solution(mesh):
    placed = (
        P(("ep", "tp"), None),
        P(),
        P(("ep", "tp"), None),
        P(("ep", "tp"), None),
        P("tp", None, None),
        P("tp", None, None),
        P("tp", None, None),
        P(),
        P(),
        P(),
    )
    return jax.shard_map(
        per_device,
        mesh=mesh,
        in_specs=placed,
        out_specs=(P(("ep", "tp"), None), P()),
        check_vma=False,
    )
```

time: 143 us -> 57.4 us (0.40)
  blocking collectives: 91.8 us -> 0 us
  Pallas kernels: 0 us -> 52.2 us
  local copies, waits for them, and re-layouts: 20 us -> 4.4 us
  matrix products: 13.5 us -> 0 us
  other arithmetic: 11.6 us -> 0 us
  starting transfers between devices: 4.5 us -> 0 us
    psum x1 -> x0, blocking collectives: 59.9 us -> none  [per_device(): total_counts = lax.psum(local_counts, ('ep', 'tp'))]
    pallas_call x0 -> x1, Pallas kernels: none -> 52.2 us  [per_device(): pl.pallas_call(functools.partial(kernel, n, eps, cap), out_shape=(jax.Sha...]
    all_to_all x1 -> x0, blocking collectives: 31.9 us -> none  [per_device(): lax.all_to_all(outgoing, 'tp', split_axis=0, concat_axis=0, tiled=True)]
    dot_general x4 -> x0, matrix products: 13.5 us -> none  [the longest x2 9.71 us: gated_mlp(): return jnp.dot(hidden, w_down, preferred_element_type=jnp.float32)]
    reduce_sum x4 -> x0, other arithmetic: 8.39 us -> none  [the longest x1 5.72 us: per_device(): routed = jnp.sum(gates[:, :, None] * per_copy.astype(jnp.float32), axis=1)]
    gather x1 -> x0, local copies, waits for them, and re-layouts: 5.2 us -> none  [per_device(): flat_returned[destination].reshape(count_rows, top_count, feature_count)]
    all_to_all x1 -> x0, starting transfers between devices: 4.5 us -> none  [per_device(): lax.all_to_all(result, 'tp', split_axis=0, concat_axis=0, tiled=True)]
    scatter x1 -> x0, local copies, waits for them, and re-layouts: 4.44 us -> none  [per_device(): jnp.zeros((groups * capacity, feature_count), jnp.bfloat16).at[destination]]
  transfers between devices with their start and end apart: 1 -> 0, of which waited for: 0 -> 0; matrix products, arithmetic and copies ran while one was open for 2% -> 0% of each run, Pallas kernels for 0% -> 0%
where the time goes in v1:
time: 57.4 us; the launch traced here: 57.2 us
  Pallas kernels  52.2 us (91%)
  local copies, waits for them, and re-layouts  4.4 us (8%)
  between operations  0.64 us (1%)
    pallas_call x1, Pallas kernels, per_device(): pl.pallas_call(functools.partial(kernel, n, eps, cap), out_shape=(jax.Sha...  52.2 us
    unnamed x3, local copies, waits for them, and re-layouts  4.4 us

profile of v1, /device:TPU:0, one launch (start us, length us, event | category | flops | bytes accessed | tf_op | source)
XLA Modules:
  0.0 57.2 jit_solution(4646248283457184650)
XLA Ops:
  0.6 1.4 %copy.12.gates = f32[128,2]{1,0:T(8,128)} copy(f32[128,2]{0,1:T(2,128)} %param.13) | data formatting | bytes 2048 | tf_op args[3]
  2.0 52.2 %shard_map.113 = (bf16[128,2048]{1,0:T(8,128)(2,1)}, f32[1,8]{1,0:T(1,128)}) custom-call(bf16[128,2048]{1,0:T(8,128)(2,1)} %tokens.1, s32[2,128]{1,0:T(2,128)} %bitcast.4, f32[128,2]{1,0:T(8,128)} %copy.12.gates, f32[1,2048]{1,0:T(1,128)} %bitcast.3, bf16[1,2048,512]{2,1,0:T(8,128)(2,1)} %expert_gate.1, bf16[1,2048,512]{2,1,0:T(8,128)(2,1)} %expert_up.1, ...), custom_call_target="tpu_custom_call" | custom-call | tf_op jit(solution)/shard_map/pallas_call | solution.py:350
  54.2 1.9 %copy.15 = bf16[128,2048]{1,0:T(8,128)(2,1)} copy(bf16[128,2048]{1,0:T(8,128)(2,1)} %get-tuple-element.8) | data formatting | bytes 1048576
  56.1 1.1 %copy.16 = f32[8]{0:T(128)} copy(f32[8]{0:T(128)} %bitcast.5) | data formatting | bytes 64

commit v2 on v1

--- a/solution.py
+++ b/solution.py
@@ -15,7 +15,7 @@
     n,
     eps,
     cap,
-    tokens,
+    tokens_hbm,
     routes,
     gates,
     gain,
@@ -27,6 +27,7 @@
     shared_down,
     out,
     load,
+    tokens,
     blocks,
     group_routes,
     every_routes,
@@ -68,6 +69,15 @@
         nd = nx + 4 * (1 - 2 * ybit)
         order = [me, sib, nx, nx + across, ny, ny + across, nd, nd + across]
 
+    barrier = pltpu.get_barrier_semaphore()
+    planes = [lax.rem(here + i, eps) for i in range(1, eps)]
+    for peer in order[1:]:
+        pl.semaphore_signal(barrier, inc=1, device_id={"tp": peer})
+    for plane in planes:
+        pl.semaphore_signal(barrier, inc=1, device_id={"ep": plane})
+    own_tokens = pltpu.make_async_copy(tokens_hbm, tokens, own_sem.at[1])
+    own_tokens.start()
+
     weights = [
         pltpu.make_async_copy(src, dst, weight_sem.at[i])
         for i, (src, dst) in enumerate(
@@ -86,12 +96,6 @@
     own_routes = pltpu.make_async_copy(routes, group_routes.at[me], own_sem.at[0])
     own_routes.start()
 
-    barrier = pltpu.get_barrier_semaphore()
-    planes = [lax.rem(here + i, eps) for i in range(1, eps)]
-    for peer in order[1:]:
-        pl.semaphore_signal(barrier, inc=1, device_id={"tp": peer})
-    for plane in planes:
-        pl.semaphore_signal(barrier, inc=1, device_id={"ep": plane})
     pl.semaphore_wait(barrier, n - 1 + eps - 1)
 
     pending = []
@@ -124,6 +128,7 @@
         ref = part(blocks.at[slot], piece)
         pltpu.make_async_copy(ref, ref, token_recv.at[slot, piece]).wait()
 
+    own_tokens.wait()
     if relay:
         send(tokens, 0, me, nx, 0)
         send(tokens, 1, me, ny, 1)
@@ -153,38 +158,37 @@
         up_part = jnp.dot(values, up_ref[...], preferred_element_type=F32)
         return (gate_part * (1.0 / (1.0 + jnp.exp(-gate_part))) * up_part).astype(BF16)
 
-    def gather(number):
-        for g in range(chunk):
-            source = order[number * chunk + g]
-            named = group_routes[source]
-            member = (named[0:1] == me) | (named[1:2] == me)
-            count = jnp.dot(
-                jnp.broadcast_to(member.astype(F32), (8, rows)).astype(BF16),
-                earlier,
-                preferred_element_type=F32,
-            )[0:1].astype(jnp.int32)
-            slot = jnp.where(member, count, -1)
-            pick = (row_in_slot == slot).astype(F32).astype(BF16)
-            held = tokens[...] if number * chunk + g == 0 else blocks[source]
-            taken = jnp.dot(pick, held, preferred_element_type=F32)
-            rows_in[g * cap : (g + 1) * cap, :] = normed_of(taken)
+    def gather(i, at):
+        source = order[i]
+        named = group_routes[source]
+        member = (named[0:1] == me) | (named[1:2] == me)
+        count = jnp.dot(
+            jnp.broadcast_to(member.astype(F32), (8, rows)).astype(BF16),
+            earlier,
+            preferred_element_type=F32,
+        )[0:1].astype(jnp.int32)
+        slot = jnp.where(member, count, -1)
+        pick = (row_in_slot == slot).astype(F32).astype(BF16)
+        held = tokens[...] if i == 0 else blocks[source]
+        taken = jnp.dot(pick, held, preferred_element_type=F32)
+        rows_in[at * cap : (at + 1) * cap, :] = normed_of(taken)
 
     tile = 512
 
-    def expert(number):
-        hidden[...] = gated(rows_in[...], w_gate, w_up)
+    def expert(members):
+        count = len(members) * cap
+        hidden[:count] = gated(rows_in[:count], w_gate, w_up)
         for at in range(0, width, tile):
             value = jnp.dot(
-                hidden[...], w_down[:, at : at + tile], preferred_element_type=F32
+                hidden[:count], w_down[:, at : at + tile], preferred_element_type=F32
             ).astype(BF16)
-            for g in range(chunk):
+            for g, i in enumerate(members):
                 piece = value[g * cap : (g + 1) * cap]
-                if number * chunk + g == 0:
+                if i == 0:
                     returned[me, :, at : at + tile] = piece
                 else:
-                    results[number * chunk + g, :, at : at + tile] = piece
-        for g in range(chunk):
-            i = number * chunk + g
+                    results[i, :, at : at + tile] = piece
+        for i in members:
             if i == 0:
                 continue
             copy = pltpu.make_async_remote_copy(
@@ -213,9 +217,10 @@
         pending.append(copy)
 
     if relay:
+        gather(0, 0)
         landed(sib, 0)
         landed(sib, 1)
-        gather(0)
+        gather(1, 1)
         landed(nx, 0)
         send(blocks.at[nx], 0, nx, ny, 6)
         send(blocks.at[nx], 0, nx, sib, 7)
@@ -224,38 +229,44 @@
         send(blocks.at[ny], 1, ny, sib, 9)
         for copy in weights[:3]:
             copy.wait()
-        expert(0)
+        expert([0, 1])
         landed(nx, 1)
         send(blocks.at[nx], 1, nx, sib, 10)
         landed(ny, 0)
         send(blocks.at[ny], 0, ny, sib, 11)
-        for number in (1, 2):
-            landed(order[2 * number + 1], 0)
-            landed(order[2 * number + 1], 1)
-            gather(number)
-            expert(number)
+        gather(2, 0)
+        gather(4, 1)
+        expert([2, 4])
+        for i, at in ((3, 0), (5, 1)):
+            landed(order[i], 0)
+            landed(order[i], 1)
+            gather(i, at)
+        expert([3, 5])
         landed(nd, 0)
         send(blocks.at[nd], 0, nd, sib, 12)
         landed(nd, 1)
         send(blocks.at[nd], 1, nd, sib, 13)
+        gather(6, 0)
         landed(order[7], 0)
         landed(order[7], 1)
-        gather(3)
-        expert(3)
+        gather(7, 1)
+        expert([6, 7])
     else:
         for copy in weights[:3]:
             copy.wait()
         for number in range(n // chunk):
-            for source in order[max(1, number * chunk) : (number + 1) * chunk]:
-                landed(source, 0)
-                landed(source, 1)
-            gather(number)
-            expert(number)
+            members = list(range(number * chunk, (number + 1) * chunk))
+            for i in members:
+                if i > 0:
+                    landed(order[i], 0)
+                    landed(order[i], 1)
+                gather(i, i % chunk)
+            expert(members)
 
     for copy in weights[3:]:
         copy.wait()
-    rows_in[...] = normed_of(tokens[...].astype(F32))
-    shared = gated(rows_in[...], s_gate, s_up)
+    rows_in[:rows] = normed_of(tokens[...].astype(F32))
+    shared = gated(rows_in[:rows], s_gate, s_up)
     for at in range(0, width, tile):
         total[:, at : at + tile] = jnp.dot(
             shared, s_down[:, at : at + tile], preferred_element_type=F32
@@ -296,13 +307,16 @@
     )
     load[...] = counts[0:1, :] * (n / (rows * 2 * n * eps))
 
-    gate_of = [gates[:, k : k + 1] for k in range(2)]
-    for number in range(n // chunk):
-        sources = order[number * chunk : (number + 1) * chunk]
-        for g, source in enumerate(sources):
-            if number * chunk + g > 0:
-                ref = returned.at[source]
-                pltpu.make_async_copy(ref, ref, result_recv.at[source]).wait()
+    columns = jnp.transpose(jnp.broadcast_to(gates[0:1], (8, rows))), jnp.transpose(
+        jnp.broadcast_to(gates[1:2], (8, rows))
+    )
+    gate_of = [column[:, 0:1] for column in columns]
+    if relay:
+        parts = [[0, 1], [2, 4], [3, 5], [6], [7]]
+    else:
+        parts = [list(range(at, at + chunk)) for at in range(0, n, chunk)]
+    for members in parts:
+        sources = [order[i] for i in members]
         picks = [
             jnp.transpose(
                 jnp.concatenate(
@@ -311,7 +325,11 @@
             ).astype(BF16)
             for slot in slots
         ]
-        last = number == n // chunk - 1
+        for i, source in zip(members, sources):
+            if i > 0:
+                ref = returned.at[source]
+                pltpu.make_async_copy(ref, ref, result_recv.at[source]).wait()
+        last = members is parts[-1]
         for at in range(0, width, tile):
             back = jnp.concatenate([returned[source, :, at : at + tile] for source in sources], axis=0)
             value = total[:, at : at + tile]
@@ -324,6 +342,17 @@
 
     for copy in pending:
         copy.wait_send()
+
+
+def write_out(mixed, load, mixed_out, load_out, sem):
+    copies = [
+        pltpu.make_async_copy(mixed, mixed_out, sem.at[0]),
+        pltpu.make_async_copy(load, load_out, sem.at[1]),
+    ]
+    for copy in copies:
+        copy.start()
+    for copy in copies:
+        copy.wait()
 
 
 def per_device(
@@ -350,12 +379,13 @@
     mixed, load = pl.pallas_call(
         functools.partial(kernel, n, eps, cap),
         out_shape=(
-            jax.ShapeDtypeStruct((rows, width), BF16),
-            jax.ShapeDtypeStruct((1, n), F32),
+            pltpu.VMEM((rows, width), BF16),
+            pltpu.VMEM((1, n), F32),
         ),
-        in_specs=[vmem] * 4 + [hbm] * 6,
+        in_specs=[hbm] + [vmem] * 3 + [hbm] * 6,
         out_specs=(vmem, vmem),
         scratch_shapes=[
+            pltpu.VMEM((rows, width), BF16),
             pltpu.VMEM((n, rows, width), BF16),
             pltpu.VMEM((n, top, rows), jnp.int32),
             pltpu.VMEM((eps, n, top, rows), jnp.int32),
@@ -371,7 +401,7 @@
             pltpu.VMEM(shared_up.shape, BF16),
             pltpu.VMEM(shared_down.shape, BF16),
             dma((6,)),
-            dma((1,)),
+            dma((2,)),
             dma((n - 1,)),
             dma((n,)),
             dma((max(1, eps - 1),)),
@@ -381,11 +411,13 @@
             dma((n,)),
             dma((n,)),
         ],
-        compiler_params=pltpu.CompilerParams(collective_id=0, has_side_effects=True),
+        compiler_params=pltpu.CompilerParams(
+            collective_id=0, has_side_effects=True
+        ),
     )(
         tokens,
         routes.T,
-        gates,
+        gates.T,
         norm_gain.reshape(1, width),
         expert_gate,
         expert_up,
@@ -394,6 +426,17 @@
         shared_up,
         shared_down,
     )
+    mixed, load = pl.pallas_call(
+        write_out,
+        out_shape=(
+            jax.ShapeDtypeStruct((rows, width), BF16),
+            jax.ShapeDtypeStruct((1, n), F32),
+        ),
+        in_specs=[vmem] * 2,
+        out_specs=(hbm, hbm),
+        scratch_shapes=[dma((2,))],
+        compiler_params=pltpu.CompilerParams(vmem_limit_bytes=1 << 20),
+    )(mixed, load)
     return mixed, load.reshape(n)
 
 

time: 57.4 us -> 50.4 us (0.88)
  local copies, waits for them, and re-layouts: 4.4 us -> 0 us
  Pallas kernels: 52.2 us -> 49.2 us
    unnamed x3 -> x0, local copies, waits for them, and re-layouts: 4.4 us -> none
    pallas_call x1 -> x2, Pallas kernels: 52.2 us -> 49.2 us  [the longest x1 48.4 us: per_device(): pl.pallas_call(functools.partial(kernel, n, eps, cap), out_shape=(pltpu.V...]
where the time goes in v2:
time: 50.4 us; the launch traced here: 49.8 us
  Pallas kernels  49.2 us (98%)
  between operations  0.64 us (1%)
    pallas_call x1, Pallas kernels, per_device(): pl.pallas_call(functools.partial(kernel, n, eps, cap), out_shape=(pltpu.V...  48.4 us

profile of v2, /device:TPU:0, one launch (start us, length us, event | category | flops | bytes accessed | tf_op | source)
XLA Modules:
  0.0 49.8 jit_solution(12965407211597116402)
XLA Ops:
  0.6 48.4 %shard_map.113 = (bf16[128,2048]{1,0:T(8,128)(2,1)S(1)}, f32[1,8]{1,0:T(1,128)S(1)}) custom-call(bf16[128,2048]{1,0:T(8,128)(2,1)} %tokens_hbm.1, s32[2,128]{1,0:T(2,128)} %bitcast.5, f32[2,128]{1,0:T(2,128)} %bitcast.6, f32[1,2048]{1,0:T(1,128)} %bitcast.4, bf16[1,2048,512]{2,1,0:T(8,128)(2,1)} %expert_gate.1, bf16[1,2048,512]{2,1,0:T(8,128)(2,1)} %expert_up.1, ...), custom_call_target="tpu_custom_call" | custom-call | tf_op jit(solution)/shard_map/pallas_call | solution.py:379
  49.0 0.8 %shard_map.114 = (bf16[128,2048]{1,0:T(8,128)(2,1)}, f32[1,8]{1,0:T(1,128)}) custom-call(bf16[128,2048]{1,0:T(8,128)(2,1)S(1)} %get-tuple-element.6.mixed, f32[1,8]{1,0:T(1,128)S(1)} %get-tuple-element.7.load), custom_call_target="tpu_custom_call" | custom-call | tf_op jit(solution)/shard_map/pallas_call | solution.py:429
